TPU v7x, 32 devices: a whole 2x2x4 slice. The times are simulated.
32 devices in a mesh: sp: 8 (over z, y), tp: 4 (over x, core).
Axes of the slice: x: 2, y: 2, z: 4, core: 2. Of those that a mesh axis runs over, the one named last changes fastest.
Arguments:
- tokens: bfloat16 [2048, 4096], P(('sp', 'tp')), may hold values from -6 to 6, as said below
- query_one: bfloat16 [4096, 1024], P('sp', 'tp'), may hold values from -0.125 to 0.125
- query_two: bfloat16 [4096, 1024], P('sp', 'tp'), may hold values from -0.125 to 0.125
- key_one: bfloat16 [4096, 1024], P('sp', 'tp'), may hold values from -0.125 to 0.125
- key_two: bfloat16 [4096, 1024], P('sp', 'tp'), may hold values from -0.125 to 0.125
- value_weight: bfloat16 [4096, 2048], P('sp', 'tp'), may hold values from -0.09375 to 0.09375
- out_weight: bfloat16 [2048, 4096], P('tp', 'sp'), may hold values from -0.125 to 0.125
- lambdas: float32 [8], P('tp'), may hold values from 0.3 to 0.8
- head_gain: float32 [256], replicated, may hold values from 0.1 to 1.9
Outputs:
- layer_out: bfloat16 [2048, 4096], P(('sp', 'tp'))
Inputs may be any that keep to these rules, and one draw needn't show every extreme that they name: `tokens`: the features' mean changes between 16 equal spans of the sequence.
All inputs are finite; a program needn't handle non-finite values.
Results may differ from a plain program's by a relative error of at most 0.013.
The roundings to bfloat16 on the way count: a program that leaves them out, or rounds other values in their place, can miss the bound.
Values may be sent and summed in bfloat16 or wider, within the bound.
No kernel may reach another device: no remote copies, remote signals or barrier semaphores. Data moves between devices by JAX's collectives and lax.ppermute only.
A program may use at most 128 MiB of HBM per device.

v0:
```python
import jax
import jax.numpy as jnp
from jax import lax
from jax.sharding import PartitionSpec as P

QK = 128
V = 256
ROPE_BASE = 500000.0
EPS_NORM = 0.02


def rotate(values, positions):
    half_dim = values.shape[-1] // 2
    inverse = 1.0 / ROPE_BASE ** (
        jnp.arange(0, 2 * half_dim, 2, dtype=jnp.float32) / (2 * half_dim)
    )
    angles = positions.astype(jnp.float32)[:, None] * inverse[None, :]
    cos_part = jnp.cos(angles)[:, None, :]
    sin_part = jnp.sin(angles)[:, None, :]
    first_half = values[..., :half_dim]
    second_half = values[..., half_dim:]
    return jnp.concatenate(
        [
            first_half * cos_part - second_half * sin_part,
            second_half * cos_part + first_half * sin_part,
        ],
        axis=-1,
    )


def unchanged(carried):
    return carried


def on_device(
    tokens, query_one, query_two, key_one, key_two, value_weight, out_weight, lambdas, head_gain
):
    tp_count = lax.axis_size("tp")
    sp_index = lax.axis_index("sp")
    own_rows = tokens.shape[0]
    local_len = own_rows * tp_count
    half_len = local_len // 2
    heads_here = lambdas.shape[0]
    gathered = lax.all_gather(tokens, "tp", axis=0, tiled=True)
    row_ids = jnp.arange(local_len, dtype=jnp.int32)
    query_pos = sp_index * local_len + row_ids
    pieces = (
        lax.all_gather(query_one, "sp", axis=0, tiled=True),
        lax.all_gather(query_two, "sp", axis=0, tiled=True),
        lax.all_gather(key_one, "sp", axis=0, tiled=True),
        lax.all_gather(key_two, "sp", axis=0, tiled=True),
        lax.all_gather(value_weight, "sp", axis=0, tiled=True),
    )
    projected = tuple(
        (
            jnp.dot(gathered, weight_piece, preferred_element_type=jnp.float32)
            for weight_piece in pieces
        )
    )

    def turned(product):
        return rotate(product.reshape(local_len, heads_here, QK), query_pos).astype(jnp.bfloat16)

    q_one = turned(projected[0])
    q_two = turned(projected[1])
    k_one = turned(projected[2]).reshape(local_len, heads_here * QK)
    k_two = turned(projected[3]).reshape(local_len, heads_here * QK)
    values = projected[4].astype(jnp.bfloat16)
    scale = QK ** (-0.5)
    pieces = (
        lax.all_gather(k_one, "sp", axis=0, tiled=True),
        lax.all_gather(k_two, "sp", axis=0, tiled=True),
        lax.all_gather(values, "sp", axis=0, tiled=True),
    )
    key_count = pieces[0].shape[0]
    global_ids = jnp.arange(key_count, dtype=jnp.int32)
    shard_ids = global_ids // local_len
    within = global_ids % local_len
    key_pos = shard_ids * local_len + within
    key_sets = (
        pieces[0].reshape(key_count, heads_here, QK),
        pieces[1].reshape(key_count, heads_here, QK),
    )
    value_rows = pieces[2].reshape(key_count, heads_here, V)
    row_tops = jnp.full((2, heads_here, local_len), -1e30, jnp.float32)
    totals = jnp.zeros((2, heads_here, local_len), jnp.float32)
    accums = jnp.zeros((2, heads_here, local_len, V), jnp.float32)
    new_parts = []
    for segment in range(2):
        low_row = segment * half_len
        seg_pos = query_pos[low_row : low_row + half_len]
        queries = (q_one[low_row : low_row + half_len], q_two[low_row : low_row + half_len])
        carried = (
            row_tops[:, :, low_row : low_row + half_len],
            totals[:, :, low_row : low_row + half_len],
            accums[:, :, low_row : low_row + half_len],
        )

        def update(carried, queries=queries, seg_pos=seg_pos):
            allowed = key_pos[None, :] <= seg_pos[:, None]
            out_tops, out_totals, out_accums = ([], [], [])
            for map_index in range(2):
                scores = (
                    jnp.einsum(
                        "qhd,khd->hqk",
                        queries[map_index],
                        key_sets[map_index],
                        preferred_element_type=jnp.float32,
                    )
                    * scale
                )
                masked = jnp.where(allowed[None], scores, -1e30)
                old_top = carried[0][map_index]
                new_top = jnp.maximum(old_top, jnp.max(masked, axis=-1))
                exp_weights = jnp.where(allowed[None], jnp.exp(scores - new_top[..., None]), 0.0)
                new_total = jnp.sum(exp_weights, axis=-1)
                new_accum = jnp.einsum(
                    "hqk,khv->hqv",
                    exp_weights.astype(jnp.bfloat16),
                    value_rows,
                    preferred_element_type=jnp.float32,
                )
                out_tops.append(new_top)
                out_totals.append(new_total)
                out_accums.append(new_accum)
            return (jnp.stack(out_tops), jnp.stack(out_totals), jnp.stack(out_accums))

        needed = jnp.min(key_pos) <= jnp.max(seg_pos)
        new_parts.append(lax.cond(needed, update, unchanged, carried))
    row_tops, totals, accums = tuple(
        (
            jnp.concatenate([new_part[member] for new_part in new_parts], axis=2)
            for member in range(3)
        )
    )
    map_outputs = accums / totals[..., None]
    mixed_out = map_outputs[0] - lambdas[:, None, None] * map_outputs[1]
    scaled = (
        mixed_out
        * lax.rsqrt(jnp.mean(mixed_out * mixed_out, axis=-1, keepdims=True) + EPS_NORM)
        * head_gain
    )
    attended = scaled.astype(jnp.bfloat16)
    weight_piece = lax.all_gather(out_weight, "sp", axis=1, tiled=True)
    shaped = weight_piece.reshape(heads_here, V, weight_piece.shape[1])
    partial_terms = jnp.einsum("hqv,hvd->qd", attended, shaped, preferred_element_type=jnp.float32)
    summed = lax.psum_scatter(
        partial_terms.astype(jnp.bfloat16), "tp", scatter_dimension=0, tiled=True
    )
    return summed


def solution(mesh):
    in_specs = (
        P(("sp", "tp"), None),
        P("sp", "tp"),
        P("sp", "tp"),
        P("sp", "tp"),
        P("sp", "tp"),
        P("sp", "tp"),
        P("tp", "sp"),
        P("tp"),
        P(),
    )
    out_specs = P(("sp", "tp"), None)
    return jax.shard_map(
        on_device, mesh=mesh, in_specs=in_specs, out_specs=out_specs, check_vma=False
    )
```

profile of v0, /device:TPU:0, one launch (start us, length us, event | category | flops | bytes accessed | tf_op | source)
XLA Modules:
  0.0 554.6 jit_solution(14938328671323246360)
XLA Ops:
  6.5 0.7 all-gather.11.cloned.1.call-update
  7.3 0.7 all-gather.25.cloned.1.call-update
  8.1 0.7 all-gather.19.cloned.1.call-update
  8.8 0.5 all-gather.21.cloned.1.call-update
  9.4 0.5 all-gather.13.cloned.1.call-update
  10.5 23.7 %all-gather.11.cloned.1.call-done = bf16[256,4096]{1,0:T(8,128)(2,1)} async-done(((bf16[64,4096]{1,0:T(8,128)(2,1)}), bf16[256,4096]{1,0:T(8,128)(2,1)}) %all-gather.11.cloned.1.call-update) | async-done | bytes 2097168 | tf_op jit(solution)/shard_map/all_gather | solution.py:44
  34.2 74.9 %all-gather.25.cloned.1.call-done = bf16[4096,512]{1,0:T(8,128)(2,1)} async-done(((bf16[512,512]{1,0:T(8,128)(2,1)}), bf16[4096,512]{1,0:T(8,128)(2,1)}) %all-gather.25.cloned.1.call-update) | async-done | bytes 4194320 | tf_op jit(solution)/shard_map/all_gather | solution.py:52
  109.2 4.8 convolution_convert_fusion
  114.3 44.6 %all-gather.19.cloned.1.call-done = bf16[4096,256]{1,0:T(8,128)(2,1)} async-done(((bf16[512,256]{1,0:T(8,128)(2,1)}), bf16[4096,256]{1,0:T(8,128)(2,1)}) %all-gather.19.cloned.1.call-update) | async-done | bytes 2097168 | tf_op jit(solution)/shard_map/all_gather | solution.py:49
  159.0 2.5 fusion.74
  161.5 47.1 %all-gather.21.cloned.1.call-done = bf16[4096,256]{1,0:T(8,128)(2,1)} async-done(((bf16[512,256]{1,0:T(8,128)(2,1)}), bf16[4096,256]{1,0:T(8,128)(2,1)}) %all-gather.21.cloned.1.call-update) | async-done | bytes 2097168 | tf_op jit(solution)/shard_map/all_gather | solution.py:51
  208.6 2.5 fusion.75
  211.1 47.1 %all-gather.13.cloned.1.call-done = bf16[4096,256]{1,0:T(8,128)(2,1)} async-done(((bf16[512,256]{1,0:T(8,128)(2,1)}), bf16[4096,256]{1,0:T(8,128)(2,1)}) %all-gather.13.cloned.1.call-update) | async-done | bytes 2097168 | tf_op jit(solution)/shard_map/all_gather | solution.py:48
  258.2 2.5 fusion.72
  260.7 47.1 %all-gather.15.cloned.1.call-done = bf16[4096,256]{1,0:T(8,128)(2,1)} async-done(((bf16[512,256]{1,0:T(8,128)(2,1)}), bf16[4096,256]{1,0:T(8,128)(2,1)}) %all-gather.15.cloned.1.call-update) | async-done | bytes 2097168 | tf_op jit(solution)/shard_map/all_gather | solution.py:50
  307.8 2.5 fusion.73
  310.5 0.7 pad_maximum_fusion.7
  311.3 0.7 pad_maximum_fusion.5
  312.0 0.5 all-gather.29.cloned.1.call-update
  312.6 0.7 fusion.70
  313.3 1.2 slice_reduce_fusion.1
  316.8 40.8 %all-gather.27.cloned.1.call-done = bf16[2048,512]{1,0:T(8,128)(2,1)} async-done(((bf16[256,512]{1,0:T(8,128)(2,1)}), bf16[2048,512]{1,0:T(8,128)(2,1)}) %all-gather.27.cloned.1.call-update) | async-done | bytes 2097168 | tf_op jit(solution)/shard_map/all_gather | solution.py:73
  357.6 4.0 reshape.172
  361.6 36.0 %all-gather.23.cloned.1.call-done = bf16[2048,256]{0,1:T(8,128)(2,1)} async-done(((bf16[256,256]{0,1:T(8,128)(2,1)}), bf16[2048,256]{0,1:T(8,128)(2,1)}) %all-gather.23.cloned.1.call-update) | async-done | bytes 1048592 | tf_op jit(solution)/shard_map/all_gather | solution.py:72
  397.6 40.5 %all-gather.17.cloned.1.call-done = bf16[2048,256]{0,1:T(8,128)(2,1)} async-done(((bf16[256,256]{0,1:T(8,128)(2,1)}), bf16[2048,256]{0,1:T(8,128)(2,1)}) %all-gather.17.cloned.1.call-update) | async-done | bytes 1048592 | tf_op jit(solution)/shard_map/all_gather | solution.py:71
  438.1 8.6 %conditional.2 = (f32[2,2,128]{2,1,0:T(2,128)S(1)}, f32[2,2,128,256]{3,2,1,0:T(8,128)}) conditional(s32[]{:T(128)} %convert_element_type.52, () %tuple.21, (s32[2048]{0:T(1024)S(1)}, s32[128]{0:T(128)S(1)}, bf16[256,2,128]{0,2,1:T(8,128)(2,1)S(1)}, bf16[2048,2,128]{0,2,1:T(8,128)(2,1)}, bf16[256,2,128]{0,2,1:T(8,128)(2,1)S(1)}, ...), branch_computations={%region_2.3_spmd, %region_3.8_spmd} | conditional | flops 815136768 | bytes 35283528 | solution.py:129
  438.3 0.8 copy.20
  439.1 1.9 select_reduce_fusion.1
  441.0 0.8 copy.22
  441.8 2.1 fusion.5
  443.9 0.7 fusion.8
  444.6 0.7 fusion.11
  445.3 0.8 pad_maximum_fusion
  446.1 0.6 fusion.7
  446.7 10.4 %conditional.3 = (f32[2,2,128]{2,1,0:T(2,128)S(1)}, f32[2,2,128,256]{3,2,1,0:T(8,128)}) conditional(s32[]{:T(128)} %convert_element_type.57, () %tuple.23, (s32[2048]{0:T(1024)S(1)}, s32[128]{0:T(128)}, bf16[256,2,128]{0,2,1:T(8,128)(2,1)}, bf16[2048,2,128]{0,2,1:T(8,128)(2,1)}, bf16[256,2,128]{0,2,1:T(8,128)(2,1)S(1)}, ...), branch_computations={%region_9.10_spmd, %region_10.15_spmd} | conditional | flops 815136768 | bytes 35283528 | solution.py:129
  446.9 0.9 broadcast_compare_fusion.1
  447.8 1.7 copy.25
  449.5 1.9 select_reduce_fusion.3
  451.4 0.8 copy.27
  452.2 2.1 fusion.31
  454.3 0.7 fusion.34
  455.0 0.7 fusion.37
  455.7 0.8 pad_maximum_fusion.2
  456.5 0.6 fusion.33
  457.1 1.4 maximum_divide_fusion
  458.8 54.9 %all-gather.29.cloned.1.call-done = bf16[512,4096]{1,0:T(8,128)(2,1)} async-done(((bf16[512,512]{1,0:T(8,128)(2,1)}), bf16[512,4096]{1,0:T(8,128)(2,1)}) %all-gather.29.cloned.1.call-update) | async-done | bytes 4194320 | tf_op jit(solution)/shard_map/all_gather | solution.py:144
  513.7 4.8 fusion.52
  518.5 29.5 %reduce-scatter.2.cloned.1.call-done = bf16[64,4096]{1,0:T(8,128)(2,1)} async-done(((bf16[256,4096]{1,0:T(8,128)(2,1)}), bf16[64,4096]{1,0:T(8,128)(2,1)}) %reduce-scatter.2.cloned.1.call-update) | async-done | bytes 524304 | tf_op jit(solution)/shard_map/reduce_scatter | solution.py:147
  (49 shorter events, 2.0 us)
Async XLA Ops:
  6.5 27.7 %all-gather.11.cloned.1.call-start = ((), (), s32[]{:S(2)}) async-start(), calls=%async_computation.1 | async-start | bytes 2621440 | tf_op jit(solution)/shard_map/all_gather | solution.py:44
  7.3 101.9 %all-gather.25.cloned.1.call-start = ((), (), s32[]{:S(2)}) async-start(), calls=%async_computation.8 | async-start | bytes 4718592 | tf_op jit(solution)/shard_map/all_gather | solution.py:52
  8.0 150.9 %all-gather.19.cloned.1.call-start = ((), (), s32[]{:S(2)}) async-start(), calls=%async_computation.5 | async-start | bytes 2359296 | tf_op jit(solution)/shard_map/all_gather | solution.py:49
  8.7 199.9 %all-gather.21.cloned.1.call-start = ((), (), s32[]{:S(2)}) async-start(), calls=%async_computation.6 | async-start | bytes 2359296 | tf_op jit(solution)/shard_map/all_gather | solution.py:51
  9.3 248.9 %all-gather.13.cloned.1.call-start = ((), (), s32[]{:S(2)}) async-start(), calls=%async_computation.2 | async-start | bytes 2359296 | tf_op jit(solution)/shard_map/all_gather | solution.py:48
  9.9 297.9 %all-gather.15.cloned.1.call-start = ((), (), s32[]{:S(2)}) async-start(), calls=%async_computation.3 | async-start | bytes 2359296 | tf_op jit(solution)/shard_map/all_gather | solution.py:50
  10.5 347.1 %all-gather.27.cloned.1.call-start = ((), (), s32[]{:S(2)}) async-start(), calls=%async_computation.9 | async-start | bytes 2359296 | tf_op jit(solution)/shard_map/all_gather | solution.py:73
  34.2 124.7 %copy-start = (bf16[256,4096]{1,0:T(8,128)(2,1)S(1)}, bf16[256,4096]{1,0:T(8,128)(2,1)}, u32[]{:S(2)}) copy-start(bf16[256,4096]{1,0:T(8,128)(2,1)} %all-gather.11.cloned.1.call-done) | copy-start | bytes 6291460
  114.0 283.7 %all-gather.23.cloned.1.call-start = ((), (), s32[]{:S(2)}) async-start(), calls=%async_computation.7 | async-start | bytes 1179648 | tf_op jit(solution)/shard_map/all_gather | solution.py:72
  311.2 126.9 %all-gather.17.cloned.1.call-start = ((), (), s32[]{:S(2)}) async-start(), calls=%async_computation.4 | async-start | bytes 1179648 | tf_op jit(solution)/shard_map/all_gather | solution.py:71
  312.0 201.7 %all-gather.29.cloned.1.call-start = ((), (), s32[]{:S(2)}) async-start(), calls=%async_computation.10 | async-start | bytes 4718592 | tf_op jit(solution)/shard_map/all_gather | solution.py:144
  312.5 235.5 %reduce-scatter.2.cloned.1.call-start = ((), (), s32[]{:S(2)}) async-start(), calls=%async_computation.11 | async-start | bytes 2621440 | tf_op jit(solution)/shard_map/reduce_scatter | solution.py:147
  316.8 121.3 %copy-start.5 = (bf16[256,2,128]{0,2,1:T(8,128)(2,1)}, bf16[256,2,128]{0,2,1:T(8,128)(2,1)S(1)}, u32[]{:S(2)}) copy-start(bf16[256,2,128]{0,2,1:T(8,128)(2,1)S(1)} %pad_maximum_fusion.4) | copy-start | bytes 393220
  438.1 3.7 copy-start.1
  441.8 2.1 copy-start.3
  446.9 5.3 copy-start.2
  452.2 2.1 copy-start.4
  457.1 1.5 copy-start.6
  457.1 56.6 %copy-start.7 = (f32[256]{0:T(256)S(1)}, f32[256]{0:T(256)}, u32[]{:S(2)}) copy-start(f32[256]{0:T(256)} %param.21) | copy-start | bytes 3076
Sparse Core Ops, SparseCore 0:
  8.9 25.2 all-gather.10
  36.3 72.7 all-gather.24
  111.3 47.6 all-gather.18
  160.9 47.6 all-gather.20
  210.6 47.5 all-gather.12
  260.2 47.6 all-gather.14
  310.0 47.6 all-gather.26
  359.7 37.9 all-gather.22
  399.7 38.3 all-gather.16
  440.0 73.6 all-gather.28
  518.7 29.3 reduce-scatter.1
where the time goes:
time: 555 us
  waiting for transfers between devices  490 us (88%)
  matrix products  30.4 us (5%)
  between operations  15.7 us (3%)
  other arithmetic  9.28 us (2%)
  local copies, waits for them, and re-layouts  7.99 us (1%)
    all_gather x1, waiting for transfers between devices, on_device(): lax.all_gather(value_weight, 'sp', axis=0, tiled=True)  74.9 us
    all_gather x1, waiting for transfers between devices, on_device(): weight_piece = lax.all_gather(out_weight, 'sp', axis=1, tiled=True)  54.9 us
    all_gather x1, waiting for transfers between devices, on_device(): lax.all_gather(key_two, 'sp', axis=0, tiled=True)  47.1 us
    all_gather x1, waiting for transfers between devices, on_device(): lax.all_gather(key_one, 'sp', axis=0, tiled=True)  47.1 us
    all_gather x1, waiting for transfers between devices, on_device(): lax.all_gather(query_one, 'sp', axis=0, tiled=True)  47.1 us
    all_gather x1, waiting for transfers between devices, on_device(): lax.all_gather(query_two, 'sp', axis=0, tiled=True)  44.6 us
    all_gather x1, waiting for transfers between devices, on_device(): lax.all_gather(values, 'sp', axis=0, tiled=True)  40.8 us
    all_gather x1, waiting for transfers between devices, on_device(): lax.all_gather(k_one, 'sp', axis=0, tiled=True)  40.5 us
  transfers between devices with their start and end apart: 11, of which 11 were waited for; matrix products, arithmetic and copies ran while one was open for 8% of the time, Pallas kernels for 0%

commit v1 on v0

--- a/solution.py
+++ b/solution.py
@@ -68,7 +68,9 @@
     values = projected[4].astype(jnp.bfloat16)
     scale = QK ** (-0.5)
     pieces = (
-        lax.all_gather(k_one, "sp", axis=0, tiled=True),
+        jnp.concatenate(
+            lax.all_to_all(jnp.stack([k_one] * lax.axis_size("sp")), "sp", 0, 0), axis=0
+        ),
         lax.all_gather(k_two, "sp", axis=0, tiled=True),
         lax.all_gather(values, "sp", axis=0, tiled=True),
     )

time: 555 us -> 525 us (0.946)
  waiting for transfers between devices: 490 us -> 456 us
    all_gather x1 -> x0, waiting for transfers between devices: 40.5 us -> none  [on_device(): lax.all_gather(k_one, 'sp', axis=0, tiled=True)]
    all_to_all x0 -> x1, waiting for transfers between devices: none -> 34.8 us  [on_device(): lax.all_to_all(jnp.stack([k_one] * lax.axis_size('sp')), 'sp', 0, 0)]
    all_gather x1, waiting for transfers between devices: 40.8 us -> 10.6 us  [on_device(): lax.all_gather(values, 'sp', axis=0, tiled=True)]
where the time goes in v1:
time: 525 us
  waiting for transfers between devices  456 us (87%)
  matrix products  30.4 us (6%)
  between operations  16.3 us (3%)
  local copies, waits for them, and re-layouts  9.56 us (2%)
  other arithmetic  8.63 us (2%)
    all_gather x1, waiting for transfers between devices, on_device(): lax.all_gather(value_weight, 'sp', axis=0, tiled=True)  74.9 us
    all_gather x1, waiting for transfers between devices, on_device(): weight_piece = lax.all_gather(out_weight, 'sp', axis=1, tiled=True)  55.8 us
    all_gather x1, waiting for transfers between devices, on_device(): lax.all_gather(key_two, 'sp', axis=0, tiled=True)  47.1 us
    all_gather x1, waiting for transfers between devices, on_device(): lax.all_gather(key_one, 'sp', axis=0, tiled=True)  47.1 us
    all_gather x1, waiting for transfers between devices, on_device(): lax.all_gather(query_one, 'sp', axis=0, tiled=True)  47.1 us
    all_gather x1, waiting for transfers between devices, on_device(): lax.all_gather(query_two, 'sp', axis=0, tiled=True)  44.6 us
    all_gather x1, waiting for transfers between devices, on_device(): lax.all_gather(k_two, 'sp', axis=0, tiled=True)  36 us
    all_to_all x1, waiting for transfers between devices, on_device(): lax.all_to_all(jnp.stack([k_one] * lax.axis_size('sp')), 'sp', 0, 0)  34.8 us
  transfers between devices with their start and end apart: 11, of which 11 were waited for; matrix products, arithmetic and copies ran while one was open for 8% of the time, Pallas kernels for 0%

profile of v1, /device:TPU:0, one launch (start us, length us, event | category | flops | bytes accessed | tf_op | source)
XLA Modules:
  0.0 524.7 jit_solution(8355254251615333372)
XLA Ops:
  6.5 0.7 all-gather.10.cloned.1.call-update
  7.3 0.7 all-gather.22.cloned.1.call-update
  8.1 0.7 all-gather.16.cloned.1.call-update
  9.4 0.5 all-gather.12.cloned.1.call-update
  10.5 23.7 %all-gather.10.cloned.1.call-done = bf16[256,4096]{1,0:T(8,128)(2,1)} async-done(((bf16[64,4096]{1,0:T(8,128)(2,1)}), bf16[256,4096]{1,0:T(8,128)(2,1)}) %all-gather.10.cloned.1.call-update) | async-done | bytes 2097168 | tf_op jit(solution)/shard_map/all_gather | solution.py:44
  34.2 74.9 %all-gather.22.cloned.1.call-done = bf16[4096,512]{1,0:T(8,128)(2,1)} async-done(((bf16[512,512]{1,0:T(8,128)(2,1)}), bf16[4096,512]{1,0:T(8,128)(2,1)}) %all-gather.22.cloned.1.call-update) | async-done | bytes 4194320 | tf_op jit(solution)/shard_map/all_gather | solution.py:52
  109.2 4.8 convolution_convert_fusion
  114.3 44.6 %all-gather.16.cloned.1.call-done = bf16[4096,256]{1,0:T(8,128)(2,1)} async-done(((bf16[512,256]{1,0:T(8,128)(2,1)}), bf16[4096,256]{1,0:T(8,128)(2,1)}) %all-gather.16.cloned.1.call-update) | async-done | bytes 2097168 | tf_op jit(solution)/shard_map/all_gather | solution.py:49
  159.0 2.5 fusion.74
  161.5 47.1 %all-gather.18.cloned.1.call-done = bf16[4096,256]{1,0:T(8,128)(2,1)} async-done(((bf16[512,256]{1,0:T(8,128)(2,1)}), bf16[4096,256]{1,0:T(8,128)(2,1)}) %all-gather.18.cloned.1.call-update) | async-done | bytes 2097168 | tf_op jit(solution)/shard_map/all_gather | solution.py:51
  208.6 2.5 fusion.75
  211.1 47.1 %all-gather.12.cloned.1.call-done = bf16[4096,256]{1,0:T(8,128)(2,1)} async-done(((bf16[512,256]{1,0:T(8,128)(2,1)}), bf16[4096,256]{1,0:T(8,128)(2,1)}) %all-gather.12.cloned.1.call-update) | async-done | bytes 2097168 | tf_op jit(solution)/shard_map/all_gather | solution.py:48
  258.2 2.5 fusion.72
  260.7 47.1 %all-gather.14.cloned.1.call-done = bf16[4096,256]{1,0:T(8,128)(2,1)} async-done(((bf16[512,256]{1,0:T(8,128)(2,1)}), bf16[4096,256]{1,0:T(8,128)(2,1)}) %all-gather.14.cloned.1.call-update) | async-done | bytes 2097168 | tf_op jit(solution)/shard_map/all_gather | solution.py:50
  307.8 2.5 fusion.73
  310.5 0.7 pad_maximum_fusion.7
  311.3 0.7 all-gather.26.cloned.1.call-update
  312.0 1.1 stack.39
  313.0 3.6 all-to-all-start
  316.6 0.7 fusion.70
  317.4 1.2 slice_reduce_fusion.1
  321.3 34.8 %all-to-all-done = bf16[8,256,256]{1,2,0:T(8,128)(2,1)S(1)} async-done(((bf16[8,256,256]{1,2,0:T(8,128)(2,1)}), bf16[8,256,256]{1,2,0:T(8,128)(2,1)S(1)}, u32[]{:S(2)}, u32[]{:S(2)}) %all-to-all-start) | async-done | bytes 1048608 | tf_op jit(solution)/shard_map/all_to_all | solution.py:72
  356.1 0.6 copy.30
  357.2 10.6 %all-gather.24.cloned.1.call-done = bf16[2048,512]{1,0:T(8,128)(2,1)} async-done(((bf16[256,512]{1,0:T(8,128)(2,1)}), bf16[2048,512]{1,0:T(8,128)(2,1)}) %all-gather.24.cloned.1.call-update) | async-done | bytes 2097168 | tf_op jit(solution)/shard_map/all_gather | solution.py:75
  367.8 4.0 reshape.169
  371.9 36.0 %all-gather.20.cloned.1.call-done = bf16[2048,256]{0,1:T(8,128)(2,1)} async-done(((bf16[256,256]{0,1:T(8,128)(2,1)}), bf16[2048,256]{0,1:T(8,128)(2,1)}) %all-gather.20.cloned.1.call-update) | async-done | bytes 1048592 | tf_op jit(solution)/shard_map/all_gather | solution.py:74
  407.9 8.6 %conditional.2 = (f32[2,2,128]{2,1,0:T(2,128)S(1)}, f32[2,2,128,256]{3,2,1,0:T(8,128)}) conditional(s32[]{:T(128)} %convert_element_type.53, () %tuple.21, (s32[2048]{0:T(1024)S(1)}, s32[128]{0:T(128)S(1)}, bf16[256,2,128]{0,2,1:T(8,128)(2,1)S(1)}, bf16[2048,2,128]{0,2,1:T(8,128)(2,1)S(1)}, bf16[256,2,128]{0,2,1:T(8,128)(2,1)S(1)}, ...), branch_computations={%region_2.3_spmd, %region_3.8_spmd} | conditional | flops 815136768 | bytes 31089196 | solution.py:131
  408.1 0.8 copy.31
  408.8 1.5 select_reduce_fusion.1
  410.3 0.8 copy.33
  411.1 2.5 fusion.5
  413.6 0.7 fusion.8
  414.3 0.7 fusion.11
  415.0 0.8 pad_maximum_fusion
  415.9 0.6 fusion.7
  416.4 9.6 %conditional.3 = (f32[2,2,128]{2,1,0:T(2,128)S(1)}, f32[2,2,128,256]{3,2,1,0:T(8,128)}) conditional(s32[]{:T(128)} %convert_element_type.58, () %tuple.23, (s32[2048]{0:T(1024)S(1)}, s32[128]{0:T(128)}, bf16[256,2,128]{0,2,1:T(8,128)(2,1)}, bf16[2048,2,128]{0,2,1:T(8,128)(2,1)S(1)}, bf16[256,2,128]{0,2,1:T(8,128)(2,1)S(1)}, ...), branch_computations={%region_9.10_spmd, %region_10.15_spmd} | conditional | flops 815136768 | bytes 31089196 | solution.py:131
  416.6 0.8 broadcast_compare_fusion.1
  417.5 1.7 copy.36
  419.1 1.5 select_reduce_fusion.3
  420.8 2.4 fusion.31
  423.2 0.7 fusion.34
  423.9 0.7 fusion.37
  424.6 0.8 pad_maximum_fusion.2
  425.5 0.6 fusion.33
  426.1 1.4 maximum_divide_fusion
  427.7 55.8 %all-gather.26.cloned.1.call-done = bf16[512,4096]{1,0:T(8,128)(2,1)} async-done(((bf16[512,512]{1,0:T(8,128)(2,1)}), bf16[512,4096]{1,0:T(8,128)(2,1)}) %all-gather.26.cloned.1.call-update) | async-done | bytes 4194320 | tf_op jit(solution)/shard_map/all_gather | solution.py:146
  483.6 4.8 fusion.52
  488.4 29.5 %reduce-scatter.2.cloned.1.call-done = bf16[64,4096]{1,0:T(8,128)(2,1)} async-done(((bf16[256,4096]{1,0:T(8,128)(2,1)}), bf16[64,4096]{1,0:T(8,128)(2,1)}) %reduce-scatter.2.cloned.1.call-update) | async-done | bytes 524304 | tf_op jit(solution)/shard_map/reduce_scatter | solution.py:149
  (47 shorter events, 3.1 us)
Async XLA Ops:
  6.5 27.7 %all-gather.10.cloned.1.call-start = ((), (), s32[]{:S(2)}) async-start(), calls=%async_computation.2 | async-start | bytes 2621440 | tf_op jit(solution)/shard_map/all_gather | solution.py:44
  7.3 101.9 %all-gather.22.cloned.1.call-start = ((), (), s32[]{:S(2)}) async-start(), calls=%async_computation.8 | async-start | bytes 4718592 | tf_op jit(solution)/shard_map/all_gather | solution.py:52
  8.0 150.9 %all-gather.16.cloned.1.call-start = ((), (), s32[]{:S(2)}) async-start(), calls=%async_computation.5 | async-start | bytes 2359296 | tf_op jit(solution)/shard_map/all_gather | solution.py:49
  8.7 199.9 %all-gather.18.cloned.1.call-start = ((), (), s32[]{:S(2)}) async-start(), calls=%async_computation.6 | async-start | bytes 2359296 | tf_op jit(solution)/shard_map/all_gather | solution.py:51
  9.3 248.9 %all-gather.12.cloned.1.call-start = ((), (), s32[]{:S(2)}) async-start(), calls=%async_computation.3 | async-start | bytes 2359296 | tf_op jit(solution)/shard_map/all_gather | solution.py:48
  9.9 297.9 %all-gather.14.cloned.1.call-start = ((), (), s32[]{:S(2)}) async-start(), calls=%async_computation.4 | async-start | bytes 2359296 | tf_op jit(solution)/shard_map/all_gather | solution.py:50
  10.5 357.4 %all-gather.24.cloned.1.call-start = ((), (), s32[]{:S(2)}) async-start(), calls=%async_computation.9 | async-start | bytes 2359296 | tf_op jit(solution)/shard_map/all_gather | solution.py:75
  34.2 124.7 %copy-start = (bf16[256,4096]{1,0:T(8,128)(2,1)S(1)}, bf16[256,4096]{1,0:T(8,128)(2,1)}, u32[]{:S(2)}) copy-start(bf16[256,4096]{1,0:T(8,128)(2,1)} %all-gather.10.cloned.1.call-done) | copy-start | bytes 6291460
  114.0 293.9 %all-gather.20.cloned.1.call-start = ((), (), s32[]{:S(2)}) async-start(), calls=%async_computation.7 | async-start | bytes 1179648 | tf_op jit(solution)/shard_map/all_gather | solution.py:74
  311.2 172.4 %all-gather.26.cloned.1.call-start = ((), (), s32[]{:S(2)}) async-start(), calls=%async_computation.10 | async-start | bytes 4718592 | tf_op jit(solution)/shard_map/all_gather | solution.py:146
  313.0 43.1 %all-to-all-start = ((bf16[8,256,256]{1,2,0:T(8,128)(2,1)}), bf16[8,256,256]{1,2,0:T(8,128)(2,1)S(1)}, u32[]{:S(2)}, u32[]{:S(2)}) async-start(bf16[8,256,256]{1,2,0:T(8,128)(2,1)} %stack.39), calls=%async_computation | async-start | bytes 2097152 | tf_op jit(solution)/shard_map/all_to_all | solution.py:72
  316.6 201.3 %reduce-scatter.2.cloned.1.call-start = ((), (), s32[]{:S(2)}) async-start(), calls=%async_computation.11 | async-start | bytes 2621440 | tf_op jit(solution)/shard_map/reduce_scatter | solution.py:149
  321.3 86.6 %copy-start.3 = (bf16[256,2,128]{0,2,1:T(8,128)(2,1)}, bf16[256,2,128]{0,2,1:T(8,128)(2,1)S(1)}, u32[]{:S(2)}) copy-start(bf16[256,2,128]{0,2,1:T(8,128)(2,1)S(1)} %pad_maximum_fusion.4) | copy-start | bytes 393220
  411.1 2.5 copy-start.1
  420.8 2.5 copy-start.2
  426.0 1.5 copy-start.4
  426.1 57.5 %copy-start.5 = (f32[256]{0:T(256)S(1)}, f32[256]{0:T(256)}, u32[]{:S(2)}) copy-start(f32[256]{0:T(256)} %param.21) | copy-start | bytes 3076
Sparse Core Ops, SparseCore 0:
  8.9 25.2 all-gather.9
  36.3 72.7 all-gather.21
  111.3 47.6 all-gather.15
  160.9 47.6 all-gather.17
  210.6 47.5 all-gather.11
  260.2 47.6 all-gather.13
  310.0 57.8 all-gather.23
  369.9 37.9 all-gather.19
  409.9 73.6 all-gather.25
  488.5 29.3 reduce-scatter.1
